TPU v7x, 32 devices: a whole 2x2x4 slice. The times are simulated.
32 devices in a mesh: dp: 4 (over y, x), kv: 4 (over z), tp: 2 (over core).
Axes of the slice: x: 2, y: 2, z: 4, core: 2. Of those that a mesh axis runs over, the one named last changes fastest.
Arguments:
- piece_tokens: bfloat16 [256, 2048], P(('dp', 'kv')), parts along dimension 0, may hold values from -6 to 6
- dec_tokens: bfloat16 [192, 4, 2048], P(('dp', 'kv')), parts along dimension 0, may hold values from -6 to 6
- norm_gain: float32 [2048], replicated, may hold values from 0.1 to 1.9
- query_weight: bfloat16 [2048, 1024], P(None, 'tp'), may hold values from -0.375 to 0.375
- key_weight: bfloat16 [2048, 256], P(None, 'tp'), may hold values from -0.125 to 0.125
- value_weight: bfloat16 [2048, 256], P(None, 'tp'), may hold values from -0.125 to 0.125
- gate_weight: bfloat16 [2048, 8], P(None, 'tp'), may hold values from -0.125 to 0.125
- gate_bias: float32 [8], P('tp'), may hold values from 3.4 to 11
- out_weight: bfloat16 [1024, 2048], P('tp'), may hold values from -0.1875 to 0.1875
- out_gain: float32 [2048], replicated, may hold values from 0.1 to 1.9
- past_keys: bfloat16 [4096, 2, 128], P(('dp', 'kv'), 'tp'), parts along dimension 0, may hold values from -41 to 41
- past_values: bfloat16 [4096, 2, 128], P(('dp', 'kv'), 'tp'), parts along dimension 0, may hold values from -6 to 6
- past_gate: float32 [8, 4096], P('tp', ('dp', 'kv')), parts along dimension 1, may hold values from -1024 to 0
- dec_keys: bfloat16 [192, 512, 2, 128], P(('dp', 'kv'), None, 'tp'), parts along dimension 0, may hold values from -41 to 41
- dec_values: bfloat16 [192, 512, 2, 128], P(('dp', 'kv'), None, 'tp'), parts along dimension 0, may hold values from -6 to 6
- dec_gate: float32 [192, 8, 512], P(('dp', 'kv'), 'tp'), parts along dimension 0, may hold values from -512 to 0
- dec_lengths: int32 [192], P(('dp', 'kv')), parts along dimension 0, may hold values from 1 to 512, as said below
Outputs:
- piece_out: bfloat16 [256, 2048], P(('dp', 'kv')), parts along dimension 0
- dec_out: bfloat16 [192, 4, 2048], P(('dp', 'kv')), parts along dimension 0
There are 4 independent parts, one for each index of `dp`. A program takes and returns all parts, laid end to end along the dimension named above; an argument that names none is the same for every part. Nothing has to cross between parts.
Inputs may be any that keep to these rules, and one draw needn't show every extreme that they name: `dec_lengths`: some decoding sequence has all 512 slots live in every draw.
All inputs are finite; a program needn't handle non-finite values.
Results may differ from a plain program's by a relative error of at most 0.015.
Values may be sent and summed in bfloat16 or wider, within the bound.
A program may use at most 64 MiB of HBM per device.

v0:
```python
import jax
import jax.numpy as jnp
from jax import lax
from jax.sharding import PartitionSpec as P

EPS = 1e-06


def rms_scale(source, scale_gain):
    widened = source.astype(jnp.float32)
    return (
        widened * lax.rsqrt(jnp.mean(widened * widened, axis=-1, keepdims=True) + EPS) * scale_gain
    )


def body(
    piece_tokens,
    dec_tokens,
    norm_gain,
    query_weight,
    key_weight,
    value_weight,
    gate_weight,
    gate_bias,
    out_weight,
    out_gain,
    past_keys,
    past_values,
    past_gate,
    dec_keys,
    dec_values,
    dec_gate,
    dec_lengths,
):
    piece_rows = piece_tokens.shape[0]
    model_width = piece_tokens.shape[1]
    kv_local = past_keys.shape[1]
    head_dim = past_keys.shape[2]
    heads_local = gate_bias.shape[0]
    group_size = heads_local // kv_local
    score_scale = head_dim ** (-0.5)
    seq_count = dec_tokens.shape[0]
    new_count = dec_tokens.shape[1]
    kv_count = lax.axis_size("kv")
    position = lax.axis_index("kv")
    all_rows = jnp.concatenate(
        [piece_tokens, dec_tokens.reshape(seq_count * new_count, model_width)], axis=0
    )
    normed = rms_scale(all_rows, norm_gain).astype(jnp.bfloat16)
    queries = jnp.dot(normed, query_weight, preferred_element_type=jnp.float32).astype(jnp.bfloat16)
    key_rows = jnp.dot(normed, key_weight, preferred_element_type=jnp.float32).astype(jnp.bfloat16)
    value_rows = jnp.dot(normed, value_weight, preferred_element_type=jnp.float32).astype(
        jnp.bfloat16
    )
    log_gates = jax.nn.log_sigmoid(
        jnp.dot(normed, gate_weight, preferred_element_type=jnp.float32) + gate_bias
    )
    piece_queries = queries[:piece_rows]
    piece_keys = key_rows[:piece_rows].reshape(piece_rows, kv_local, head_dim)
    piece_values = value_rows[:piece_rows].reshape(piece_rows, kv_local, head_dim)
    local_run = jnp.cumsum(log_gates[:piece_rows], axis=0)
    gathered_run = lax.all_gather(local_run, "kv", axis=0, tiled=True)
    shard_run = gathered_run.reshape(kv_count, piece_rows, heads_local)
    totals = shard_run[:, -1]
    before = jnp.cumsum(totals, axis=0) - totals
    piece_run = (shard_run + before[:, None, :]).reshape(kv_count * piece_rows, heads_local)
    own_run = lax.dynamic_slice_in_dim(piece_run, position * piece_rows, piece_rows, 0)
    key_place = position * piece_rows + jnp.arange(piece_rows)
    gate_groups = jnp.moveaxis(past_gate.reshape(kv_local, group_size, -1), 1, 0)
    own_groups = jnp.moveaxis(own_run.reshape(piece_rows, kv_local, group_size), 2, 0)
    shard_queries = lax.all_gather(piece_queries, "kv", axis=0, tiled=True)
    row_count = shard_queries.shape[0]
    query_groups = jnp.moveaxis(
        shard_queries.reshape(row_count, kv_local, group_size, head_dim), 2, 0
    )
    run_groups = jnp.moveaxis(piece_run.reshape(row_count, kv_local, group_size), 2, 0)
    row_place = jnp.arange(row_count)
    causal = key_place[None, :] <= row_place[:, None]

    def one_group(inputs):
        query_one, run_one, gate_one, key_run_one = inputs
        row_bias = run_one.T[:, :, None]
        past_scores = (
            jnp.einsum("nkd,pkd->knp", query_one, past_keys, preferred_element_type=jnp.float32)
            * score_scale
        )
        past_scores = past_scores + gate_one[:, None, :] + row_bias
        new_scores = (
            jnp.einsum("nkd,jkd->knj", query_one, piece_keys, preferred_element_type=jnp.float32)
            * score_scale
        )
        new_scores = new_scores + row_bias - key_run_one.T[:, None, :]
        new_scores = jnp.where(causal[None], new_scores, -jnp.inf)
        row_top = jnp.maximum(jnp.max(past_scores, axis=-1), jnp.max(new_scores, axis=-1))
        past_exp = jnp.exp(past_scores - row_top[..., None])
        new_exp = jnp.exp(new_scores - row_top[..., None])
        row_total = jnp.sum(past_exp, axis=-1) + jnp.sum(new_exp, axis=-1)
        summed = jnp.einsum(
            "knp,pkd->nkd",
            past_exp.astype(jnp.bfloat16),
            past_values,
            preferred_element_type=jnp.float32,
        )
        summed = summed + jnp.einsum(
            "knj,jkd->nkd",
            new_exp.astype(jnp.bfloat16),
            piece_values,
            preferred_element_type=jnp.float32,
        )
        return (summed, row_top.T, row_total.T)

    group_out, group_top, group_total = lax.map(
        one_group, (query_groups, run_groups, gate_groups, own_groups)
    )
    group_out = jnp.moveaxis(group_out, 0, 2).reshape(row_count, heads_local, head_dim)
    group_top = jnp.moveaxis(group_top, 0, 2).reshape(row_count, heads_local)
    group_total = jnp.moveaxis(group_total, 0, 2).reshape(row_count, heads_local)
    arrived = (
        lax.all_to_all(
            group_out.reshape(kv_count, piece_rows, heads_local, head_dim),
            "kv",
            split_axis=0,
            concat_axis=0,
            tiled=True,
        ),
        lax.all_to_all(
            group_top.reshape(kv_count, piece_rows, heads_local),
            "kv",
            split_axis=0,
            concat_axis=0,
            tiled=True,
        ),
        lax.all_to_all(
            group_total.reshape(kv_count, piece_rows, heads_local),
            "kv",
            split_axis=0,
            concat_axis=0,
            tiled=True,
        ),
    )
    global_top = jnp.max(arrived[1], axis=0)
    weights = jnp.exp(arrived[1] - global_top)
    row_total = jnp.sum(arrived[2] * weights, axis=0)
    piece_result = jnp.sum(arrived[0] * weights[..., None], axis=0) / row_total[..., None]
    piece_attention = piece_result.reshape(piece_rows, heads_local * head_dim).astype(jnp.bfloat16)
    dec_queries = queries[piece_rows:].reshape(seq_count, new_count, kv_local, group_size, head_dim)
    dec_new_keys = key_rows[piece_rows:].reshape(seq_count, new_count, kv_local, head_dim)
    dec_new_values = value_rows[piece_rows:].reshape(seq_count, new_count, kv_local, head_dim)
    dec_run = jnp.cumsum(log_gates[piece_rows:].reshape(seq_count, new_count, heads_local), axis=1)
    past_len = dec_keys.shape[1]
    slot_index = jnp.arange(past_len)
    last_gate = jnp.sum(
        jnp.where(slot_index[None, None, :] == (dec_lengths - 1)[:, None, None], dec_gate, 0.0),
        axis=2,
    )
    query_bias = jnp.moveaxis(dec_run.reshape(seq_count, new_count, kv_local, group_size), 1, 3)
    past_bias = last_gate.reshape(seq_count, kv_local, group_size)[..., None, None]
    dec_gate_groups = dec_gate.reshape(seq_count, kv_local, group_size, past_len)
    new_scores = (
        jnp.einsum(
            "stkgd,sukd->skgtu", dec_queries, dec_new_keys, preferred_element_type=jnp.float32
        )
        * score_scale
    )
    new_scores = new_scores + query_bias[..., None] - query_bias[..., None, :]
    new_causal = jnp.arange(new_count)[None, :] <= jnp.arange(new_count)[:, None]
    new_scores = jnp.where(new_causal, new_scores, -jnp.inf)
    new_top = jnp.max(new_scores, axis=-1)
    new_exp = jnp.exp(new_scores - new_top[..., None])
    start_dec = (
        jnp.einsum(
            "skgtu,sukd->skgtd",
            new_exp.astype(jnp.bfloat16),
            dec_new_values,
            preferred_element_type=jnp.float32,
        ),
        new_top,
        jnp.sum(new_exp, axis=-1),
    )
    block_scores = (
        jnp.einsum("stkgd,spkd->skgtp", dec_queries, dec_keys, preferred_element_type=jnp.float32)
        * score_scale
    )
    block_scores = (
        block_scores + query_bias[..., None] + past_bias - dec_gate_groups[:, :, :, None, :]
    )
    live_mask = jnp.arange(past_len)[None, :] < dec_lengths[:, None]
    block_scores = jnp.where(live_mask[:, None, None, None, :], block_scores, -jnp.inf)
    row_top = jnp.maximum(start_dec[1], jnp.max(block_scores, axis=-1))
    block_exp = jnp.exp(block_scores - row_top[..., None])
    rescale = jnp.exp(start_dec[1] - row_top)
    summed = start_dec[0] * rescale[..., None] + jnp.einsum(
        "skgtp,spkd->skgtd",
        block_exp.astype(jnp.bfloat16),
        dec_values,
        preferred_element_type=jnp.float32,
    )
    dec_attention = summed / (start_dec[2] * rescale + jnp.sum(block_exp, axis=-1))[..., None]
    dec_attention = (
        jnp.transpose(dec_attention, (0, 3, 1, 2, 4))
        .reshape(seq_count * new_count, heads_local * head_dim)
        .astype(jnp.bfloat16)
    )
    attention = jnp.concatenate([piece_attention, dec_attention], axis=0)
    partial_rows = jnp.dot(attention, out_weight, preferred_element_type=jnp.float32)
    mixed = lax.psum(partial_rows.astype(jnp.bfloat16), "tp").astype(jnp.float32)
    final_rows = rms_scale(mixed, out_gain).astype(jnp.bfloat16)
    return (
        final_rows[:piece_rows],
        final_rows[piece_rows:].reshape(seq_count, new_count, model_width),
    )


def solution(mesh):
    return jax.shard_map(
        body,
        mesh=mesh,
        in_specs=(
            P(("dp", "kv"), None),
            P(("dp", "kv"), None, None),
            P(),
            P(None, "tp"),
            P(None, "tp"),
            P(None, "tp"),
            P(None, "tp"),
            P("tp"),
            P("tp", None),
            P(),
            P(("dp", "kv"), "tp", None),
            P(("dp", "kv"), "tp", None),
            P("tp", ("dp", "kv")),
            P(("dp", "kv"), None, "tp", None),
            P(("dp", "kv"), None, "tp", None),
            P(("dp", "kv"), "tp", None),
            P(("dp", "kv")),
        ),
        out_specs=(P(("dp", "kv"), None), P(("dp", "kv"), None, None)),
        check_vma=False,
    )
```

profile of v0, /device:TPU:0, one launch (start us, length us, event | category | flops | bytes accessed | tf_op | source)
XLA Modules:
  0.0 105.0 jit_solution(5508176570152350641)
XLA Ops:
  7.2 1.1 %reshape.318 = bf16[48,2048]{1,0:T(8,128)(2,1)S(1)} reshape(bf16[12,4,2048]{2,1,0:T(4,128)(2,1)} %param.20) | data formatting | bytes 393216 | tf_op jit(solution)/shard_map/reshape | solution.py:47
  8.4 1.0 fusion.69
  9.4 1.1 %fusion.87 = f32[64,4]{0,1:T(4,128)S(1)} fusion(bf16[2048,4]{0,1:T(4,128)(2,1)} %param.25, f32[4]{0:T(128)} %param.26, f32[2048]{0:T(1024)} %param.21, f32[64]{0:T(128)S(1)} %add_rsqrt_fusion.1, bf16[48,2048]{1,0:T(8,128)(2,1)S(1)} %reshape.318, bf16[16,2048]{1,0:T(8,128)(2,1)} %param.19), kind=kOutput, calls=%fused_computation.106 | convolution fusion | flops 1968384 | bytes 288016 | tf_op jit(solution)/shard_map/dot_general | solution.py:56
  10.7 13.6 %all-gather = f32[4,16,4]{1,2,0:T(4,128)S(1)} all-gather(f32[1,16,4]{1,2,0:T(4,128)S(1)} %bitcast.224), channel_id=1, replica_groups=mesh['dp'=4,'kv'=4,'tp'=2] {'kv'}, dimensions={0}, use_global_device_ids=true | all-gather | bytes 1280 | tf_op jit(solution)/shard_map/all_gather | solution.py:62
  24.8 0.9 transpose_reshape.3
  25.6 1.4 %convolution_convert_fusion.3 = bf16[64,128]{1,0:T(8,128)(2,1)S(1)} fusion(bf16[2048,128]{1,0:T(8,128)(2,1)} %param.23, f32[2048]{0:T(1024)} %param.21, f32[64]{0:T(128)S(1)} %add_rsqrt_fusion.1, bf16[48,2048]{1,0:T(8,128)(2,1)S(1)} %reshape.318, bf16[16,2048]{1,0:T(8,128)(2,1)} %param.19), kind=kOutput, calls=%fused_computation.61 | convolution fusion | flops 34480128 | bytes 811264 | tf_op jit(solution)/shard_map/dot_general | solution.py:51
  27.1 0.3 convolution_convert_fusion.2
  27.4 0.5 convolution_convert_fusion.1
  27.9 13.1 %all_gather.6 = bf16[64,512]{1,0:T(8,128)(2,1)S(1)} all-gather(bf16[16,512]{1,0:T(8,128)(2,1)S(1)} %slice.44), channel_id=1, replica_groups=mesh['dp'=4,'kv'=4,'tp'=2] {'kv'}, dimensions={0}, use_global_device_ids=true | all-gather | bytes 81920 | tf_op jit(solution)/shard_map/all_gather | solution.py:71
  41.2 4.4 %while.15 = (s32[]{:T(128)}, f32[4,64,1,128]{3,1,2,0:T(8,128)S(1)}, f32[4,64,1]{1,2,0:T(1,128)S(1)}, f32[4,64,1]{1,2,0:T(1,128)S(1)}, bf16[4,64,1,128]{3,1,2,0:T...) while((s32[]{:T(128)}, f32[4,64,1,128]{3,1,2,0:T(8,128)S(1)}, ...), condition=%wide.region_8.9_spmd.clone, body=%wide.region_3.8_spmd.clone.sunk | while | flops 9062274 | bytes 495149 | solution.py:112
  41.4 0.3 fusion.126
  41.7 0.2 fusion.131
  41.9 0.2 fusion.129
  42.1 0.2 fusion.130
  42.5 0.3 fusion.126
  42.8 0.2 fusion.131
  43.0 0.2 fusion.129
  43.2 0.2 fusion.130
  43.6 0.3 fusion.126
  43.9 0.2 fusion.131
  44.1 0.2 fusion.129
  44.3 0.2 fusion.130
  44.7 0.3 fusion.126
  45.0 0.2 fusion.131
  45.2 0.2 fusion.129
  45.4 0.2 fusion.130
  45.7 0.6 copy.73
  46.3 3.4 %all-to-all-start.1 = ((f32[4,16,4]{1,2,0:T(4,128)}), f32[4,16,4]{1,2,0:T(4,128)S(1)}, u32[]{:S(2)}, u32[]{:S(2)}) async-start(f32[4,16,4]{1,2,0:T(4,128)} %copy.73), calls=%async_computation.1 | async-start | bytes 16384 | tf_op jit(solution)/shard_map/all_to_all | solution.py:126
  50.1 0.6 reduce_window_sum.38
  50.7 0.2 copy.78
  50.9 0.6 fusion.95
  51.6 0.4 copy.80
  52.1 2.0 %fusion.96 = (f32[12,4,4]{1,2,0:T(4,128)S(1)}, f32[12,1,4,4,512]{4,2,3,0,1:T(4,128)S(1)}) fusion(f32[12,4,512]{2,1,0:T(4,128)S(1)} %copy-done.5, f32[12,4]{1,0:T(8,128)S(1)} %select_reduce_fusion, f32[12,4,4]{1,2,0:T(4,128)S(1)} %copy.78, bf16[12,4,4,128]{3,2,1,0:T(4,128)(2,1)S(1)} %reshape.325, bf16[12,512,1,128]{3,1,2,0:T(8,128)(2,1)} %param.32, ...), kind=kOutput, calls=%fused_computation.119 | convolution fusion | flops 25755456 | bytes 2121408 | tf_op jit(solution)/shard_map/stkgd,spkd->skgtp/dot_general | solution.py:181
  54.2 0.3 fusion.77
  54.5 0.2 copy.82
  54.9 0.6 copy.75
  55.7 5.1 %all-to-all-start.2 = ((f32[4,16,4]{1,2,0:T(4,128)}), f32[4,16,4]{1,2,0:T(4,128)S(1)}, u32[]{:S(2)}, u32[]{:S(2)}) async-start(f32[4,16,4]{1,2,0:T(4,128)} %copy.75), calls=%async_computation.2 | async-start | bytes 16384 | tf_op jit(solution)/shard_map/all_to_all | solution.py:133
  60.8 1.8 %fusion.65 = bf16[12,4,1,4,128]{4,1,3,0,2:T(4,128)(2,1)S(1)} fusion(f32[12,4,4,128]{3,2,1,0:T(4,128)S(1)} %convolution_multiply_fusion.2, bf16[12,512,1,128]{3,1,2,0:T(8,128)(2,1)} %param.33, bf16[12,4,4,512]{3,1,2,0:T(4,128)(2,1)S(1)} %get-tuple-element.191, f32[12,4,4]{2,1,0:T(4,128)S(1)} %copy.84), kind=kOutput, calls=%fused_computation.59 | convolution fusion | flops 25239552 | bytes 1917696 | tf_op jit(solution)/shard_map/skgtp,spkd->skgtd/dot_general | solution.py:192
  62.6 0.7 copy.72
  63.3 3.2 %all-to-all-done.2 = f32[4,16,4]{1,2,0:T(4,128)S(1)} async-done(((f32[4,16,4]{1,2,0:T(4,128)}), f32[4,16,4]{1,2,0:T(4,128)S(1)}, u32[]{:S(2)}, u32[]{:S(2)}) %all-to-all-start.2) | async-done | bytes 1056 | tf_op jit(solution)/shard_map/all_to_all | solution.py:133
  66.5 3.3 %all-to-all-start = ((f32[4,16,4,128]{3,1,2,0:T(8,128)}), f32[4,16,4,128]{3,1,2,0:T(8,128)S(1)}, u32[]{:S(2)}, u32[]{:S(2)}) async-start(f32[4,16,4,128]{3,1,2,0:T(8,128)} %copy.72), calls=%async_computation | async-start | bytes 262144 | tf_op jit(solution)/shard_map/all_to_all | solution.py:119
  69.9 5.8 %all-to-all-done = f32[4,16,4,128]{3,1,2,0:T(8,128)S(1)} async-done(((f32[4,16,4,128]{3,1,2,0:T(8,128)}), f32[4,16,4,128]{3,1,2,0:T(8,128)S(1)}, u32[]{:S(2)}, u32[]{:S(2)}) %all-to-all-start) | async-done | bytes 131104 | tf_op jit(solution)/shard_map/all_to_all | solution.py:119
  75.9 1.2 %convolution_convert_fusion = bf16[64,2048]{1,0:T(8,128)(2,1)} fusion(bf16[512,2048]{1,0:T(8,128)(2,1)S(1)} %copy-done, bf16[48,512]{1,0:T(8,128)(2,1)S(1)} %bitcast.214, bf16[16,512]{1,0:T(8,128)(2,1)S(1)} %copy_bitcast_fusion.2), kind=kOutput, calls=%fused_computation.38 | convolution fusion | flops 134479872 | bytes 2424832 | tf_op jit(solution)/shard_map/dot_general | solution.py:205
  77.1 17.4 %all-reduce.2.cloned.1.call-done = bf16[64,2048]{1,0:T(8,128)(2,1)} async-done(((bf16[64,2048]{1,0:T(8,128)(2,1)}), bf16[64,2048]{1,0:T(8,128)(2,1)}) %all-reduce.2.cloned.1.call-update) | async-done | bytes 262160 | tf_op jit(solution)/shard_map/psum | solution.py:206
  94.6 1.1 %fusion.72 = f32[64]{0:T(128)S(1)} fusion(bf16[64,2048]{1,0:T(8,128)(2,1)} %all-reduce.2.cloned.1.call-done), kind=kLoop, calls=%fused_computation.72 | loop fusion | flops 393152 | bytes 262400 | tf_op jit(solution)/shard_map/reduce_sum | solution.py:12
  95.7 1.1 %fusion.74 = bf16[64,2048]{1,0:T(8,128)(2,1)S(1)} fusion(bf16[64,2048]{1,0:T(8,128)(2,1)} %all-reduce.2.cloned.1.call-done, f32[2048]{0:T(1024)S(1)} %copy-done.8, f32[64]{0:T(128)S(1)} %add_rsqrt_fusion), kind=kLoop, calls=%fused_computation.74 | loop fusion | flops 524288 | bytes 532736 | tf_op jit(solution)/shard_map/convert_element_type | solution.py:207
  96.8 0.6 slice.51
  97.4 0.8 reshape.331
  (100 shorter events, 3.1 us)
Async XLA Ops:
  7.2 68.7 %copy-start = (bf16[512,2048]{1,0:T(8,128)(2,1)S(1)}, bf16[512,2048]{1,0:T(8,128)(2,1)}, u32[]{:S(2)}) copy-start(bf16[512,2048]{1,0:T(8,128)(2,1)} %param.27) | copy-start | bytes 6291460
  7.2 19.8 %copy-start.4 = (bf16[16,2048]{1,0:T(8,128)(2,1)S(1)}, bf16[16,2048]{1,0:T(8,128)(2,1)}, u32[]{:S(2)}) copy-start(bf16[16,2048]{1,0:T(8,128)(2,1)} %param.19) | copy-start | bytes 196612
  7.2 19.8 %copy-start.7 = (f32[2048]{0:T(1024)S(1)}, f32[2048]{0:T(1024)}, u32[]{:S(2)}) copy-start(f32[2048]{0:T(1024)} %param.21) | copy-start | bytes 24580
  7.2 19.8 %copy-start.10 = (bf16[2048,128]{1,0:T(8,128)(2,1)S(1)}, bf16[2048,128]{1,0:T(8,128)(2,1)}, u32[]{:S(2)}) copy-start(bf16[2048,128]{1,0:T(8,128)(2,1)} %param.24) | copy-start | bytes 1572868
  24.8 2.6 %copy-start.1 = (bf16[2048,512]{1,0:T(8,128)(2,1)S(1)}, bf16[2048,512]{1,0:T(8,128)(2,1)}, u32[]{:S(2)}) copy-start(bf16[2048,512]{1,0:T(8,128)(2,1)} %param.22) | copy-start | bytes 6291460
  27.0 14.2 %copy-start.2 = (bf16[256,1,128]{2,0,1:T(8,128)(2,1)S(1)}, bf16[256,1,128]{2,0,1:T(8,128)(2,1)}, u32[]{:S(2)}) copy-start(bf16[256,1,128]{2,0,1:T(8,128)(2,1)} %param.29) | copy-start | bytes 196612
  27.0 14.2 %copy-start.3 = (bf16[256,1,128]{2,0,1:T(8,128)(2,1)S(1)}, bf16[256,1,128]{2,0,1:T(8,128)(2,1)}, u32[]{:S(2)}) copy-start(bf16[256,1,128]{2,0,1:T(8,128)(2,1)} %param.30) | copy-start | bytes 196612
  27.4 22.5 %copy-start.6 = (bf16[64,128]{1,0:T(8,128)(2,1)}, bf16[64,128]{1,0:T(8,128)(2,1)S(1)}, u32[]{:S(2)}) copy-start(bf16[64,128]{1,0:T(8,128)(2,1)S(1)} %convolution_convert_fusion.2) | copy-start | bytes 49156
  27.9 21.8 %copy-start.9 = (s32[12]{0:T(128)S(1)}, s32[12]{0:T(128)}, u32[]{:S(2)}) copy-start(s32[12]{0:T(128)} %param.35) | copy-start | bytes 148
  41.2 10.8 %copy-start.5 = (f32[12,4,512]{2,1,0:T(4,128)S(1)}, f32[12,4,512]{2,1,0:T(4,128)}, u32[]{:S(2)}) copy-start(f32[12,4,512]{2,1,0:T(4,128)} %param.34) | copy-start | bytes 294916
  46.3 9.4 %all-to-all-start.1 = ((f32[4,16,4]{1,2,0:T(4,128)}), f32[4,16,4]{1,2,0:T(4,128)S(1)}, u32[]{:S(2)}, u32[]{:S(2)}) async-start(f32[4,16,4]{1,2,0:T(4,128)} %copy.73), calls=%async_computation.1 | async-start | bytes 16384 | tf_op jit(solution)/shard_map/all_to_all | solution.py:126
  50.1 4.6 %slice-start = ((bf16[64,128]{1,0:T(8,128)(2,1)}), bf16[48,128]{1,0:T(8,128)(2,1)S(1)}, s32[]{:S(2)}) async-start(bf16[64,128]{1,0:T(8,128)(2,1)} %copy-done.6), calls=%async_computation.4 | async-start | bytes 24576 | tf_op jit(solution)/shard_map/slice | solution.py:148
  55.7 10.8 %all-to-all-start.2 = ((f32[4,16,4]{1,2,0:T(4,128)}), f32[4,16,4]{1,2,0:T(4,128)S(1)}, u32[]{:S(2)}, u32[]{:S(2)}) async-start(f32[4,16,4]{1,2,0:T(4,128)} %copy.75), calls=%async_computation.2 | async-start | bytes 16384 | tf_op jit(solution)/shard_map/all_to_all | solution.py:133
  62.6 33.1 %copy-start.8 = (f32[2048]{0:T(1024)S(1)}, f32[2048]{0:T(1024)}, u32[]{:S(2)}) copy-start(f32[2048]{0:T(1024)} %param.28) | copy-start | bytes 24580
  66.5 9.2 %all-to-all-start = ((f32[4,16,4,128]{3,1,2,0:T(8,128)}), f32[4,16,4,128]{3,1,2,0:T(8,128)S(1)}, u32[]{:S(2)}, u32[]{:S(2)}) async-start(f32[4,16,4,128]{3,1,2,0:T(8,128)} %copy.72), calls=%async_computation | async-start | bytes 262144 | tf_op jit(solution)/shard_map/all_to_all | solution.py:119
  69.8 24.7 %all-reduce.2.cloned.1.call-start = ((), (), s32[]{:S(2)}) async-start(), calls=%async_computation.3 | async-start | bytes 524288 | tf_op jit(solution)/shard_map/psum | solution.py:206
Sparse Core Ops, SparseCore 0:
  77.2 17.2 all-reduce.1
where the time goes:
time: 106 us; the launch traced here: 105 us
  blocking collectives  26.8 us (25%)
  waiting for transfers between devices  26.5 us (25%)
  between operations  14.4 us (14%)
  matrix products  12.2 us (12%)
  starting transfers between devices  11.9 us (11%)
  local copies, waits for them, and re-layouts  7.15 us (7%)
  other arithmetic  6.01 us (6%)
    psum x1, waiting for transfers between devices, body(): lax.psum(partial_rows.astype(jnp.bfloat16), 'tp').astype(jnp.float32)  17.4 us
    all_gather x1, blocking collectives, body(): gathered_run = lax.all_gather(local_run, 'kv', axis=0, tiled=True)  13.6 us
    all_gather x1, blocking collectives, body(): shard_queries = lax.all_gather(piece_queries, 'kv', axis=0, tiled=True)  13.1 us
    all_to_all x1, waiting for transfers between devices, body(): lax.all_to_all(group_out.reshape(kv_count, piece_rows, heads_local, head_...  5.81 us
    all_to_all x1, starting transfers between devices, body(): lax.all_to_all(group_total.reshape(kv_count, piece_rows, heads_local), 'k...  5.09 us
    all_to_all x1, starting transfers between devices, body(): lax.all_to_all(group_top.reshape(kv_count, piece_rows, heads_local), 'kv'...  3.44 us
    all_to_all x1, starting transfers between devices, body(): lax.all_to_all(group_out.reshape(kv_count, piece_rows, heads_local, head_...  3.33 us
    all_to_all x1, waiting for transfers between devices, body(): lax.all_to_all(group_total.reshape(kv_count, piece_rows, heads_local), 'k...  3.19 us
  transfers between devices with their start and end apart: 4, of which 3 were waited for; matrix products, arithmetic and copies ran while one was open for 8% of the time, Pallas kernels for 0%

commit v1 on v0

--- a/solution.py
+++ b/solution.py
@@ -68,7 +68,9 @@
     key_place = position * piece_rows + jnp.arange(piece_rows)
     gate_groups = jnp.moveaxis(past_gate.reshape(kv_local, group_size, -1), 1, 0)
     own_groups = jnp.moveaxis(own_run.reshape(piece_rows, kv_local, group_size), 2, 0)
-    shard_queries = lax.all_gather(piece_queries, "kv", axis=0, tiled=True)
+    shard_queries = jnp.concatenate(
+        lax.all_to_all(jnp.stack([piece_queries] * lax.axis_size("kv")), "kv", 0, 0), axis=0
+    )
     row_count = shard_queries.shape[0]
     query_groups = jnp.moveaxis(
         shard_queries.reshape(row_count, kv_local, group_size, head_dim), 2, 0

time: 106 us -> 101 us (0.953)
  blocking collectives: 26.8 us -> 12.5 us
  waiting for transfers between devices: 26.5 us -> 30.9 us
  starting transfers between devices: 11.9 us -> 16.2 us
    all_gather x1 -> x0, blocking collectives: 13.1 us -> none  [body(): shard_queries = lax.all_gather(piece_queries, 'kv', axis=0, tiled=True)]
    all_to_all x0 -> x1, starting transfers between devices: none -> 6.34 us  [body(): lax.all_to_all(jnp.stack([piece_queries] * lax.axis_size('kv')), 'kv', 0, 0)]
    all_to_all x1, waiting for transfers between devices: 0.01 us -> 4.58 us  [body(): lax.all_to_all(group_top.reshape(kv_count, piece_rows, heads_local), 'kv'...]
    all_to_all x1, starting transfers between devices: 5.09 us -> 3.25 us  [body(): lax.all_to_all(group_total.reshape(kv_count, piece_rows, heads_local), 'k...]
    dot_general x1, matrix products: 0.52 us -> 2.18 us  [body(): jnp.dot(normed, query_weight, preferred_element_type=jnp.float32)]
    all_gather x1, blocking collectives: 13.6 us -> 12.5 us  [body(): gathered_run = lax.all_gather(local_run, 'kv', axis=0, tiled=True)]
    dot_general x1, matrix products: 1.37 us -> 0.29 us  [body(): jnp.dot(normed, key_weight, preferred_element_type=jnp.float32)]
  transfers between devices with their start and end apart: 4 -> 5, of which waited for: 3 -> 4; matrix products, arithmetic and copies ran while one was open for 8% -> 11% of each run, Pallas kernels for 0% -> 0%
where the time goes in v1:
time: 101 us; the launch traced here: 100 us
  waiting for transfers between devices  30.9 us (31%)
  starting transfers between devices  16.2 us (16%)
  between operations  14.5 us (14%)
  matrix products  12.9 us (13%)
  blocking collectives  12.5 us (12%)
  local copies, waits for them, and re-layouts  6.94 us (7%)
  other arithmetic  6.01 us (6%)
    psum x1, waiting for transfers between devices, body(): lax.psum(partial_rows.astype(jnp.bfloat16), 'tp').astype(jnp.float32)  17.4 us
    all_gather x1, blocking collectives, body(): gathered_run = lax.all_gather(local_run, 'kv', axis=0, tiled=True)  12.5 us
    all_to_all x1, starting transfers between devices, body(): lax.all_to_all(jnp.stack([piece_queries] * lax.axis_size('kv')), 'kv', 0, 0)  6.34 us
    all_to_all x1, waiting for transfers between devices, body(): lax.all_to_all(group_out.reshape(kv_count, piece_rows, heads_local, head_...  5.81 us
    all_to_all x1, waiting for transfers between devices, body(): lax.all_to_all(group_top.reshape(kv_count, piece_rows, heads_local), 'kv'...  4.58 us
    all_to_all x1, starting transfers between devices, body(): lax.all_to_all(group_out.reshape(kv_count, piece_rows, heads_local, head_...  3.33 us
    all_to_all x1, starting transfers between devices, body(): lax.all_to_all(group_top.reshape(kv_count, piece_rows, heads_local), 'kv'...  3.25 us
    all_to_all x1, starting transfers between devices, body(): lax.all_to_all(group_total.reshape(kv_count, piece_rows, heads_local), 'k...  3.25 us
  transfers between devices with their start and end apart: 5, of which 4 were waited for; matrix products, arithmetic and copies ran while one was open for 11% of the time, Pallas kernels for 0%

profile of v1, /device:TPU:0, one launch (start us, length us, event | category | flops | bytes accessed | tf_op | source)
XLA Modules:
  0.0 100.2 jit_solution(10004748126833677245)
XLA Ops:
  7.2 1.1 %reshape.317 = bf16[48,2048]{1,0:T(8,128)(2,1)S(1)} reshape(bf16[12,4,2048]{2,1,0:T(4,128)(2,1)} %param.20) | data formatting | bytes 393216 | tf_op jit(solution)/shard_map/reshape | solution.py:47
  8.4 1.0 fusion.69
  9.4 2.2 %convolution_convert_fusion.1 = bf16[64,512]{1,0:T(8,128)(2,1)S(1)} fusion(bf16[2048,512]{1,0:T(8,128)(2,1)} %param.22, f32[2048]{0:T(1024)} %param.21, f32[64]{0:T(128)S(1)} %add_rsqrt_fusion.1, bf16[48,2048]{1,0:T(8,128)(2,1)S(1)} %reshape.317, bf16[16,2048]{1,0:T(8,128)(2,1)} %param.19), kind=kOutput, calls=%fused_computation.54 | convolution fusion | flops 135168000 | bytes 2433280 | tf_op jit(solution)/shard_map/dot_general | solution.py:50
  11.6 0.6 stack.2
  12.2 6.3 %all-to-all-start = ((bf16[4,16,512]{2,1,0:T(8,128)(2,1)}), bf16[4,16,512]{2,1,0:T(8,128)(2,1)S(1)}, u32[]{:S(2)}, u32[]{:S(2)}) async-start(bf16[4,16,512]{2,1,0:T(8,128)(2,1)} %stack.2), calls=%async_computation | async-start | bytes 131072 | tf_op jit(solution)/shard_map/all_to_all | solution.py:72
  18.7 0.3 fusion.87
  19.3 12.5 %all-gather = f32[4,16,4]{1,2,0:T(4,128)S(1)} all-gather(f32[1,16,4]{1,2,0:T(4,128)S(1)} %bitcast.222), channel_id=1, replica_groups=mesh['dp'=4,'kv'=4,'tp'=2] {'kv'}, dimensions={0}, use_global_device_ids=true | all-gather | bytes 1280 | tf_op jit(solution)/shard_map/all_gather | solution.py:62
  32.2 0.3 convolution_convert_fusion.3
  32.5 1.3 %convolution_convert_fusion.2 = bf16[64,128]{1,0:T(8,128)(2,1)S(1)} fusion(bf16[2048,128]{1,0:T(8,128)(2,1)} %param.24, f32[2048]{0:T(1024)S(1)} %copy-done.6, f32[64]{0:T(128)S(1)} %add_rsqrt_fusion.1, bf16[48,2048]{1,0:T(8,128)(2,1)S(1)} %reshape.317, bf16[16,2048]{1,0:T(8,128)(2,1)S(1)} %copy-done.3), kind=kOutput, calls=%fused_computation.60 | convolution fusion | flops 34480128 | bytes 811264 | tf_op jit(solution)/shard_map/dot_general | solution.py:52
  34.1 0.6 reduce_window_sum.38
  34.7 0.2 copy.77
  34.9 0.6 fusion.95
  35.6 0.4 copy.79
  36.1 2.0 %fusion.96 = (f32[12,4,4]{1,2,0:T(4,128)S(1)}, f32[12,1,4,4,512]{4,2,3,0,1:T(4,128)S(1)}) fusion(f32[12,4,512]{2,1,0:T(4,128)S(1)} %copy-done.4, f32[12,4]{1,0:T(8,128)S(1)} %select_reduce_fusion, f32[12,4,4]{1,2,0:T(4,128)S(1)} %copy.77, bf16[12,4,4,128]{3,2,1,0:T(4,128)(2,1)S(1)} %reshape.323, bf16[12,512,1,128]{3,1,2,0:T(8,128)(2,1)} %param.32, ...), kind=kOutput, calls=%fused_computation.118 | convolution fusion | flops 25755456 | bytes 2121408 | tf_op jit(solution)/shard_map/stkgd,spkd->skgtp/dot_general | solution.py:183
  38.2 0.3 fusion.77
  38.8 4.4 %while.15 = (s32[]{:T(128)}, f32[4,64,1,128]{3,1,2,0:T(8,128)S(1)}, f32[4,64,1]{1,2,0:T(1,128)S(1)}, f32[4,64,1]{1,2,0:T(1,128)S(1)}, bf16[4,64,1,128]{3,1,2,0:T...) while((s32[]{:T(128)}, f32[4,64,1,128]{3,1,2,0:T(8,128)S(1)}, ...), condition=%wide.region_8.9_spmd.clone, body=%wide.region_3.8_spmd.clone.sunk | while | flops 9062274 | bytes 495149 | solution.py:114
  39.1 0.3 fusion.126
  39.4 0.2 fusion.131
  39.5 0.2 fusion.129
  39.8 0.2 fusion.130
  40.1 0.3 fusion.126
  40.5 0.2 fusion.131
  40.6 0.2 fusion.129
  40.9 0.2 fusion.130
  41.2 0.3 fusion.126
  41.5 0.2 fusion.131
  41.7 0.2 fusion.129
  42.0 0.2 fusion.130
  42.3 0.3 fusion.126
  42.6 0.2 fusion.131
  42.8 0.2 fusion.129
  43.0 0.2 fusion.130
  43.3 0.6 copy.72
  44.0 3.2 %all-to-all-start.2 = ((f32[4,16,4]{1,2,0:T(4,128)}), f32[4,16,4]{1,2,0:T(4,128)S(1)}, u32[]{:S(2)}, u32[]{:S(2)}) async-start(f32[4,16,4]{1,2,0:T(4,128)} %copy.72), calls=%async_computation.2 | async-start | bytes 16384 | tf_op jit(solution)/shard_map/all_to_all | solution.py:128
  47.6 0.6 copy.74
  48.2 4.6 %all-to-all-done.2 = f32[4,16,4]{1,2,0:T(4,128)S(1)} async-done(((f32[4,16,4]{1,2,0:T(4,128)}), f32[4,16,4]{1,2,0:T(4,128)S(1)}, u32[]{:S(2)}, u32[]{:S(2)}) %all-to-all-start.2) | async-done | bytes 1056 | tf_op jit(solution)/shard_map/all_to_all | solution.py:128
  52.8 3.2 %all-to-all-start.3 = ((f32[4,16,4]{1,2,0:T(4,128)}), f32[4,16,4]{1,2,0:T(4,128)S(1)}, u32[]{:S(2)}, u32[]{:S(2)}) async-start(f32[4,16,4]{1,2,0:T(4,128)} %copy.74), calls=%async_computation.3 | async-start | bytes 16384 | tf_op jit(solution)/shard_map/all_to_all | solution.py:135
  56.1 1.8 %fusion.65 = bf16[12,4,1,4,128]{4,1,3,0,2:T(4,128)(2,1)S(1)} fusion(f32[12,4,4,128]{3,2,1,0:T(4,128)S(1)} %convolution_multiply_fusion.2, bf16[12,512,1,128]{3,1,2,0:T(8,128)(2,1)} %param.33, bf16[12,4,4,512]{3,1,2,0:T(4,128)(2,1)S(1)} %get-tuple-element.191, f32[12,4,4]{2,1,0:T(4,128)S(1)} %copy.83), kind=kOutput, calls=%fused_computation.59 | convolution fusion | flops 25239552 | bytes 1917696 | tf_op jit(solution)/shard_map/skgtp,spkd->skgtd/dot_general | solution.py:194
  57.9 0.7 copy.71
  58.6 3.0 %all-to-all-done.3 = f32[4,16,4]{1,2,0:T(4,128)S(1)} async-done(((f32[4,16,4]{1,2,0:T(4,128)}), f32[4,16,4]{1,2,0:T(4,128)S(1)}, u32[]{:S(2)}, u32[]{:S(2)}) %all-to-all-start.3) | async-done | bytes 1056 | tf_op jit(solution)/shard_map/all_to_all | solution.py:135
  61.6 3.3 %all-to-all-start.1 = ((f32[4,16,4,128]{3,1,2,0:T(8,128)}), f32[4,16,4,128]{3,1,2,0:T(8,128)S(1)}, u32[]{:S(2)}, u32[]{:S(2)}) async-start(f32[4,16,4,128]{3,1,2,0:T(8,128)} %copy.71), calls=%async_computation.1 | async-start | bytes 262144 | tf_op jit(solution)/shard_map/all_to_all | solution.py:121
  65.0 5.8 %all-to-all-done.1 = f32[4,16,4,128]{3,1,2,0:T(8,128)S(1)} async-done(((f32[4,16,4,128]{3,1,2,0:T(8,128)}), f32[4,16,4,128]{3,1,2,0:T(8,128)S(1)}, u32[]{:S(2)}, u32[]{:S(2)}) %all-to-all-start.1) | async-done | bytes 131104 | tf_op jit(solution)/shard_map/all_to_all | solution.py:121
  71.0 1.2 %convolution_convert_fusion = bf16[64,2048]{1,0:T(8,128)(2,1)} fusion(bf16[512,2048]{1,0:T(8,128)(2,1)S(1)} %copy-done, bf16[48,512]{1,0:T(8,128)(2,1)S(1)} %bitcast.212, bf16[16,512]{1,0:T(8,128)(2,1)S(1)} %copy_bitcast_fusion.1), kind=kOutput, calls=%fused_computation.38 | convolution fusion | flops 134479872 | bytes 2424832 | tf_op jit(solution)/shard_map/dot_general | solution.py:207
  72.2 17.4 %all-reduce.2.cloned.1.call-done = bf16[64,2048]{1,0:T(8,128)(2,1)} async-done(((bf16[64,2048]{1,0:T(8,128)(2,1)}), bf16[64,2048]{1,0:T(8,128)(2,1)}) %all-reduce.2.cloned.1.call-update) | async-done | bytes 262160 | tf_op jit(solution)/shard_map/psum | solution.py:208
  89.7 1.1 %fusion.72 = f32[64]{0:T(128)S(1)} fusion(bf16[64,2048]{1,0:T(8,128)(2,1)} %all-reduce.2.cloned.1.call-done), kind=kLoop, calls=%fused_computation.72 | loop fusion | flops 393152 | bytes 262400 | tf_op jit(solution)/shard_map/reduce_sum | solution.py:12
  90.8 1.1 %fusion.74 = bf16[64,2048]{1,0:T(8,128)(2,1)S(1)} fusion(bf16[64,2048]{1,0:T(8,128)(2,1)} %all-reduce.2.cloned.1.call-done, f32[2048]{0:T(1024)S(1)} %copy-done.7, f32[64]{0:T(128)S(1)} %add_rsqrt_fusion), kind=kLoop, calls=%fused_computation.74 | loop fusion | flops 524288 | bytes 532736 | tf_op jit(solution)/shard_map/convert_element_type | solution.py:209
  91.9 0.6 slice.51
  92.6 0.8 reshape.329
  (106 shorter events, 3.3 us)
Async XLA Ops:
  7.2 63.9 %copy-start = (bf16[512,2048]{1,0:T(8,128)(2,1)S(1)}, bf16[512,2048]{1,0:T(8,128)(2,1)}, u32[]{:S(2)}) copy-start(bf16[512,2048]{1,0:T(8,128)(2,1)} %param.27) | copy-start | bytes 6291460
  7.2 11.5 %copy-start.3 = (bf16[16,2048]{1,0:T(8,128)(2,1)S(1)}, bf16[16,2048]{1,0:T(8,128)(2,1)}, u32[]{:S(2)}) copy-start(bf16[16,2048]{1,0:T(8,128)(2,1)} %param.19) | copy-start | bytes 196612
  7.2 11.5 %copy-start.6 = (f32[2048]{0:T(1024)S(1)}, f32[2048]{0:T(1024)}, u32[]{:S(2)}) copy-start(f32[2048]{0:T(1024)} %param.21) | copy-start | bytes 24580
  7.2 11.4 %copy-start.9 = (s32[12]{0:T(128)S(1)}, s32[12]{0:T(128)}, u32[]{:S(2)}) copy-start(s32[12]{0:T(128)} %param.35) | copy-start | bytes 148
  7.2 11.5 %copy-start.12 = (f32[4]{0:T(128)S(1)}, f32[4]{0:T(128)}, u32[]{:S(2)}) copy-start(f32[4]{0:T(128)} %param.26) | copy-start | bytes 52
  7.2 11.5 %copy-start.11 = (bf16[2048,4]{0,1:T(4,128)(2,1)S(1)}, bf16[2048,4]{0,1:T(4,128)(2,1)}, u32[]{:S(2)}) copy-start(bf16[2048,4]{0,1:T(4,128)(2,1)} %param.25) | copy-start | bytes 49156
  7.2 24.9 %copy-start.10 = (bf16[2048,128]{1,0:T(8,128)(2,1)S(1)}, bf16[2048,128]{1,0:T(8,128)(2,1)}, u32[]{:S(2)}) copy-start(bf16[2048,128]{1,0:T(8,128)(2,1)} %param.23) | copy-start | bytes 1572868
  11.6 22.3 %copy-start.8 = (f32[4,256]{1,0:T(4,128)S(1)}, f32[4,256]{1,0:T(4,128)}, u32[]{:S(2)}) copy-start(f32[4,256]{1,0:T(4,128)} %param.31) | copy-start | bytes 12292
  12.2 26.5 %all-to-all-start = ((bf16[4,16,512]{2,1,0:T(8,128)(2,1)}), bf16[4,16,512]{2,1,0:T(8,128)(2,1)S(1)}, u32[]{:S(2)}, u32[]{:S(2)}) async-start(bf16[4,16,512]{2,1,0:T(8,128)(2,1)} %stack.2), calls=%async_computation | async-start | bytes 131072 | tf_op jit(solution)/shard_map/all_to_all | solution.py:72
  18.6 17.4 %copy-start.4 = (f32[12,4,512]{2,1,0:T(4,128)S(1)}, f32[12,4,512]{2,1,0:T(4,128)}, u32[]{:S(2)}) copy-start(f32[12,4,512]{2,1,0:T(4,128)} %param.34) | copy-start | bytes 294916
  33.8 4.7 %copy-start.5 = (bf16[64,128]{1,0:T(8,128)(2,1)}, bf16[64,128]{1,0:T(8,128)(2,1)S(1)}, u32[]{:S(2)}) copy-start(bf16[64,128]{1,0:T(8,128)(2,1)S(1)} %convolution_convert_fusion.2) | copy-start | bytes 49156
  34.9 4.0 %copy-start.1 = (bf16[256,1,128]{2,0,1:T(8,128)(2,1)S(1)}, bf16[256,1,128]{2,0,1:T(8,128)(2,1)}, u32[]{:S(2)}) copy-start(bf16[256,1,128]{2,0,1:T(8,128)(2,1)} %param.29) | copy-start | bytes 196612
  34.9 4.0 %copy-start.2 = (bf16[256,1,128]{2,0,1:T(8,128)(2,1)S(1)}, bf16[256,1,128]{2,0,1:T(8,128)(2,1)}, u32[]{:S(2)}) copy-start(bf16[256,1,128]{2,0,1:T(8,128)(2,1)} %param.30) | copy-start | bytes 196612
  38.5 8.7 %slice-start = ((bf16[64,128]{1,0:T(8,128)(2,1)}), bf16[48,128]{1,0:T(8,128)(2,1)S(1)}, s32[]{:S(2)}) async-start(bf16[64,128]{1,0:T(8,128)(2,1)} %copy-done.5), calls=%async_computation.5 | async-start | bytes 24576 | tf_op jit(solution)/shard_map/slice | solution.py:150
  44.0 8.8 %all-to-all-start.2 = ((f32[4,16,4]{1,2,0:T(4,128)}), f32[4,16,4]{1,2,0:T(4,128)S(1)}, u32[]{:S(2)}, u32[]{:S(2)}) async-start(f32[4,16,4]{1,2,0:T(4,128)} %copy.72), calls=%async_computation.2 | async-start | bytes 16384 | tf_op jit(solution)/shard_map/all_to_all | solution.py:128
  52.8 8.8 %all-to-all-start.3 = ((f32[4,16,4]{1,2,0:T(4,128)}), f32[4,16,4]{1,2,0:T(4,128)S(1)}, u32[]{:S(2)}, u32[]{:S(2)}) async-start(f32[4,16,4]{1,2,0:T(4,128)} %copy.74), calls=%async_computation.3 | async-start | bytes 16384 | tf_op jit(solution)/shard_map/all_to_all | solution.py:135
  57.8 33.0 %copy-start.7 = (f32[2048]{0:T(1024)S(1)}, f32[2048]{0:T(1024)}, u32[]{:S(2)}) copy-start(f32[2048]{0:T(1024)} %param.28) | copy-start | bytes 24580
  61.6 9.2 %all-to-all-start.1 = ((f32[4,16,4,128]{3,1,2,0:T(8,128)}), f32[4,16,4,128]{3,1,2,0:T(8,128)S(1)}, u32[]{:S(2)}, u32[]{:S(2)}) async-start(f32[4,16,4,128]{3,1,2,0:T(8,128)} %copy.71), calls=%async_computation.1 | async-start | bytes 262144 | tf_op jit(solution)/shard_map/all_to_all | solution.py:121
  64.9 24.7 %all-reduce.2.cloned.1.call-start = ((), (), s32[]{:S(2)}) async-start(), calls=%async_computation.4 | async-start | bytes 524288 | tf_op jit(solution)/shard_map/psum | solution.py:208
Sparse Core Ops, SparseCore 0:
  72.4 17.2 all-reduce.1
